TPU v7x, 32 devices: a whole 2x2x4 slice. The times are simulated.
32 devices in a mesh: sp: 8 (over z, y), tp: 4 (over x, core).
Axes of the slice: x: 2, y: 2, z: 4, core: 2. Of those that a mesh axis runs over, the one named last changes fastest.
Arguments:
- skip_stream: bfloat16 [2048, 2048], P('sp', 'tp'), may hold values from -20 to 20
- narrow_lookup_matrix: bfloat16 [2048, 256], P('sp', 'tp'), may hold values from -6 to 6
- narrow_probe_matrix: bfloat16 [2048, 256], P('sp', 'tp'), may hold values from -6 to 6
- narrow_retention_logits: bfloat16 [2048, 256], P('sp', 'tp'), may hold values from -6 to 16
- broad_lookup_matrix: bfloat16 [2048, 512], P('sp', 'tp'), may hold values from -6 to 6
- broad_probe_matrix: bfloat16 [2048, 512], P('sp', 'tp'), may hold values from -6 to 6
- broad_retention_logits: bfloat16 [2048, 512], P('sp', 'tp'), may hold values from -6 to 16
- content_vectors: bfloat16 [2048, 4, 2, 128], P('sp', 'tp'), may hold values from -6 to 6
- extra_log_retention: float32 [2048, 2, 4], P('sp', None, 'tp'), may hold values from -0.7 to 0
- per_branch_scaling: bfloat16 [4, 2, 128], P('tp'), may hold values from 0.099609375 to 1.8984375
- final_projection_matrix: bfloat16 [1024, 2048], P(None, 'tp'), may hold values from -0.1875 to 0.1875
- channel_blend_scaling: bfloat16 [2048], replicated, may hold values from 0.099609375 to 1.8984375
- switch_expansion_matrix: bfloat16 [2048, 5632], P('sp', 'tp'), may hold values from -0.125 to 0.125
- content_expansion_matrix: bfloat16 [2048, 5632], P('sp', 'tp'), may hold values from -0.125 to 0.125
- convolution_kernel: bfloat16 [3, 2, 5632], P(None, None, 'tp'), may hold values from -3.5 to 3.5
- contraction_matrix: bfloat16 [5632, 2048], P('tp', 'sp'), may hold values from -0.078125 to 0.078125
Outputs:
- mixed: bfloat16 [2048, 2048], P('sp', 'tp')
All inputs are finite; a program needn't handle non-finite values.
Results may differ from a plain program's by a relative error of at most 0.011.
Values may be sent and summed in bfloat16 or wider, within the bound.
A program may use at most 64 MiB of HBM per device.

v0:
```python
import functools

import jax
import jax.numpy as jnp
from jax import lax
from jax.experimental import pallas as pl
from jax.experimental.pallas import tpu as pltpu
from jax.sharding import PartitionSpec as P

BLOCK = 64
HALO = 16
EPSILON = 1e-06
SOFTENING = 16.0
HIGHEST = lax.Precision.HIGHEST
F32 = jnp.float32
BF16 = jnp.bfloat16
NT = (((1,), (1,)), ((), ()))


def blocked(array):
    return array.reshape(array.shape[0] // BLOCK, BLOCK, array.shape[1], array.shape[2]).transpose(
        0, 2, 1, 3
    )


def local_attention(q, k, v, log_decay):
    tokens, units, key = q.shape
    query_blocks, key_blocks, value_blocks = blocked(q), blocked(k), blocked(v)
    lower = jnp.tril(jnp.ones((BLOCK, BLOCK), dtype=bool))
    inner = jnp.einsum(
        "ij,nhjd->nhid", lower.astype(F32), blocked(log_decay), precision=HIGHEST
    )
    last = inner[:, :, -1:, :]
    middle = inner[:, :, BLOCK // 2 - 1 : BLOCK // 2, :]
    scores = jnp.einsum(
        "nhid,nhjd->nhij",
        query_blocks * jnp.exp(inner - middle),
        key_blocks * jnp.exp(middle - inner),
        precision=HIGHEST,
    )
    out = jnp.einsum(
        "nhij,nhjv->nhiv", jnp.where(lower, scores, 0.0), value_blocks, precision=HIGHEST
    )
    query_carry = query_blocks * jnp.exp(inner)
    key_carry = key_blocks * jnp.exp(last - inner)
    added = jnp.einsum("nhjd,nhjv->nhvd", key_carry, value_blocks, precision=HIGHEST)
    block_logs = last[:, :, 0, :]
    before = jnp.cumsum(block_logs, axis=0) - block_logs
    state, states = jnp.zeros_like(added[0]), []
    for n in range(added.shape[0]):
        states.append(state)
        state = jnp.exp(block_logs[n])[:, None, :] * state + added[n]
    out = out + jnp.einsum("nhid,nhvd->nhiv", query_carry, jnp.stack(states), precision=HIGHEST)
    meets = query_carry * jnp.exp(before)[:, :, None, :]
    fade = jnp.exp(jnp.sum(block_logs, axis=0))

    def unblock(a):
        return a.transpose(0, 2, 1, 3).reshape(tokens, -1)

    return unblock(out), unblock(meets), state, fade


def kernel(
    n_sp, n_tp, units,
    w_ref, st_ref, out_ref0, meets_ref, gain_ref, skip_ref, proj_ref, blend_ref, taps_ref,
    mixed_ref,
    wbuf, stbuf, acc_state, heads, resid, nb, up, hid, psum, rbuf,
    own_sem, st_send, st_recv, uz_send, uz_recv, uy_send, uy_recv, cz_send, cz_recv, cy_send,
    cy_recv, h_send, h_recv, r_send, r_recv, n_send, n_recv, d_send, d_recv,
):
    s, t = lax.axis_index("sp"), lax.axis_index("tp")
    nz = n_sp // 2
    z, y = s // 2, s % 2
    q = z % 2
    mate = s + 2 - 4 * q
    side = s + 1 - 2 * y
    tok = skip_ref.shape[0]
    cols = skip_ref.shape[1]
    half = wbuf.shape[2]
    dblk = wbuf.shape[3]
    dv = out_ref0.shape[1] // units

    def rc(src, dst, ss, rs, sp, tp):
        return pltpu.make_async_remote_copy(
            src_ref=src, dst_ref=dst, send_sem=ss, recv_sem=rs,
            device_id=(sp, tp), device_id_type=pl.DeviceIdType.MESH,
        )

    bar = pltpu.get_barrier_semaphore()
    count = 0
    for o in range(1, n_sp):
        pl.semaphore_signal(bar, inc=1, device_id=(lax.rem(s + o, n_sp), t),
                            device_id_type=pl.DeviceIdType.MESH)
        count += 1
    for row in (s, mate):
        for o in range(1, n_tp):
            pl.semaphore_signal(bar, inc=1, device_id=(row, lax.rem(t + o, n_tp)),
                                device_id_type=pl.DeviceIdType.MESH)
            count += 1
    pl.semaphore_wait(bar, count)

    st = [None] + [
        rc(st_ref, stbuf.at[s], st_send.at[o], st_recv.at[o], lax.rem(s + o, n_sp), t)
        for o in range(1, n_sp)
    ]
    for o in range(1, n_sp):
        @pl.when(s + o < n_sp)
        def _(o=o):
            st[o].start()

    def zcopies(lo, width, ss, rs):
        made = []
        for o in range(1, nz):
            zz = lax.rem(z + o, nz)
            rows = pl.ds(pl.multiple_of((zz % 2) * half, HALO), half)
            made.append(rc(w_ref.at[pl.ds(lo, width), rows], wbuf.at[s, pl.ds(lo, width)],
                           ss.at[o], rs.at[o], zz * 2 + y, t))
        return made

    def ycopy(o, lo, width, ss, rs):
        if o == 0:
            rows = pl.ds(pl.multiple_of(q * half, HALO), half)
            source = w_ref.at[pl.ds(lo, width), rows]
            slot = s
        else:
            slot = lax.rem(z + nz - o, nz) * 2 + y
            source = wbuf.at[slot, pl.ds(lo, width)]
        return rc(source, wbuf.at[slot, pl.ds(lo, width)], ss.at[o], rs.at[o], side, t)

    uz = zcopies(0, 2, uz_send, uz_recv)
    uy = [ycopy(o, 0, 2, uy_send, uy_recv) for o in range(nz)]
    for copy in uz:
        copy.start()
    uy[0].start()
    own = pltpu.make_async_copy(
        w_ref.at[:, pl.ds(pl.multiple_of(q * half, HALO), half)], wbuf.at[s], own_sem
    )
    own.start()

    acc_state[...] = jnp.zeros_like(acc_state)
    for o in range(n_sp - 1, 0, -1):
        @pl.when(s - o >= 0)
        def _(o=o):
            st[o].wait_recv()
            got = stbuf[s - o].astype(F32)
            acc_state[...] = got[dv : dv + 1] * acc_state[...] + got[:dv]
    key = meets_ref.shape[1] // units
    mine = []
    for u in range(units):
        total = out_ref0[:, u * dv : (u + 1) * dv] + lax.dot_general(
            meets_ref[:, u * key : (u + 1) * key], acc_state[:, u * key : (u + 1) * key],
            NT, precision=HIGHEST, preferred_element_type=F32,
        )
        scale = lax.rsqrt(jnp.mean(total * total, axis=-1, keepdims=True) + EPSILON)
        mine.append((total * scale * gain_ref[u : u + 1, :]).astype(BF16))
    heads[t] = jnp.concatenate(mine, axis=1)
    hc = [
        rc(heads.at[t], heads.at[t], h_send.at[o], h_recv.at[o], s, lax.rem(t + o, n_tp))
        for o in range(1, n_tp)
    ]
    for copy in hc:
        copy.start()
    for copy in hc:
        copy.wait_recv()
    width = units * dv
    projected = skip_ref[...].astype(F32)
    whole_heads = jnp.concatenate([heads[i] for i in range(n_tp)], axis=1)
    projected = projected + jnp.dot(whole_heads, proj_ref[...], preferred_element_type=F32)
    resid[t] = projected.astype(BF16)
    qc = [
        rc(resid.at[t], resid.at[t], r_send.at[o], r_recv.at[o], s, lax.rem(t + o, n_tp))
        for o in range(1, n_tp)
    ]
    for copy in qc:
        copy.start()
    for copy in qc:
        copy.wait_recv()
    squares = jnp.zeros((tok, 1), F32)
    for i in range(n_tp):
        part = resid[i].astype(F32)
        squares = squares + jnp.sum(part * part, axis=1, keepdims=True)
    scale = lax.rsqrt(squares / (n_tp * cols) + EPSILON)
    for i in range(n_tp):
        piece = slice(i * cols, (i + 1) * cols)
        nb[0, HALO:, piece] = (
            resid[i].astype(F32) * scale * blend_ref[:, piece]
        ).astype(BF16)
    after = lax.rem(s + 1, n_sp)
    after_mate = after + 2 - 4 * ((after // 2) % 2)
    block = pl.ds(HALO, tok)
    tail = pl.ds(tok, HALO)
    nc = [
        rc(nb.at[0, tail], nb.at[0, pl.ds(0, HALO)], n_send.at[0], n_recv.at[0], after, t),
        rc(nb.at[0, tail], nb.at[1, pl.ds(0, HALO)], n_send.at[1], n_recv.at[1], after_mate, t),
        rc(nb.at[0, block], nb.at[1, block], n_send.at[2], n_recv.at[2], mate, t),
    ]
    for copy in nc:
        copy.start()
    cz = zcopies(2, 1, cz_send, cz_recv)
    cy = [ycopy(o, 2, 1, cy_send, cy_recv) for o in range(nz)]
    for copy in cz:
        copy.start()
    for o in range(1, nz):
        uz[o - 1].wait_recv()
        uy[o].start()
    cy[0].start()
    for copy in nc:
        copy.wait_recv()
    own.wait()
    for o in range(nz):
        uy[o].wait_recv()

    for m in range(2):
        for i in range(2):
            up[m, i] = jnp.zeros_like(up[m, i])

    group = max(1, 128 // dblk)

    def expand_add(b, carry):
        at = pl.ds(pl.multiple_of(b * group * dblk, 128), group * dblk)
        for i in range(2):
            rows = nb[i, :, at]
            for j in range(group):
                part = rows[:, j * dblk : (j + 1) * dblk]
                for m in range(2):
                    up[m, i] += lax.dot_general(
                        part, wbuf[b * group + j, m], NT, preferred_element_type=F32
                    )
        return carry

    lax.fori_loop(0, n_sp // group, expand_add, 0)
    for o in range(1, nz):
        cz[o - 1].wait_recv()
        cy[o].start()
    for i in range(2):
        first = (s if i == 0 else mate) == 0
        conv = []
        for m in range(2):
            keep = jnp.where(first, 0.0, 1.0)
            edge = up[m, i, :HALO].astype(BF16).astype(F32)
            up[m, i, :HALO] = edge * keep
            up[m, i, HALO:] = up[m, i, HALO:].astype(BF16).astype(F32)
            total = taps_ref[m * 3 : m * 3 + 1] * up[m, i, pl.ds(HALO - 2, tok)]
            total += taps_ref[m * 3 + 1 : m * 3 + 2] * up[m, i, pl.ds(HALO - 1, tok)]
            total += taps_ref[m * 3 + 2 : m * 3 + 3] * up[m, i, pl.ds(HALO, tok)]
            conv.append(total)
        value, gate = conv
        hid[pl.ds(i * tok, tok)] = (gate / (1.0 + jnp.exp(-gate)) * value).astype(BF16)
    for o in range(nz):
        cy[o].wait_recv()
    per = cols // dblk
    dc = []
    for o in range(1, n_tp + 1):
        to = lax.rem(t + o, n_tp)
        for j in range(per):
            part = jnp.dot(hid[...], wbuf[to * per + j, 2], preferred_element_type=F32).astype(BF16)
            psum[to, 0, :, j * dblk : (j + 1) * dblk] = part[:tok]
            psum[to, 1, :, j * dblk : (j + 1) * dblk] = part[tok:]
        for i in range(2):
            if i == 0 and o == n_tp:
                continue
            at = i * n_tp + o - 1
            copy = rc(psum.at[to, i], rbuf.at[at], d_send.at[at], d_recv.at[at],
                      s if i == 0 else mate, to)
            copy.start()
            dc.append((at, copy))
    total = psum[t, 0].astype(F32)
    for at, copy in dc:
        copy.wait_recv()
        total = total + rbuf[at].astype(F32)
    mixed_ref[...] = (resid[t].astype(F32) + total).astype(BF16)

    for o in range(1, n_sp):
        @pl.when(s + o < n_sp)
        def _(o=o):
            st[o].wait_send()
    for copy in uz + uy + cz + cy + hc + qc + nc + [c for _, c in dc]:
        copy.wait_send()


def local(
    n_sp, n_tp,
    skip_stream,
    narrow_lookup_matrix,
    narrow_probe_matrix,
    narrow_retention_logits,
    broad_lookup_matrix,
    broad_probe_matrix,
    broad_retention_logits,
    content_vectors,
    extra_log_retention,
    per_branch_scaling,
    final_projection_matrix,
    channel_blend_scaling,
    switch_expansion_matrix,
    content_expansion_matrix,
    convolution_kernel,
    contraction_matrix,
):
    tok, cols = skip_stream.shape
    heads = content_vectors.shape[1]
    dv = content_vectors.shape[3]
    narrow = narrow_lookup_matrix.shape[1] // heads
    broad = broad_lookup_matrix.shape[1] // heads
    units = 2 * heads

    def pair(a, b):
        a = a.astype(F32).reshape(tok, heads, narrow)
        b = b.astype(F32).reshape(tok, heads, broad)
        return a, b

    def join(a, b):
        a = jnp.pad(a, ((0, 0), (0, 0), (0, broad - narrow)))
        return jnp.stack([a, b], axis=2).reshape(tok, units, broad)

    qa, qb = pair(narrow_lookup_matrix, broad_lookup_matrix)
    query = join(qa * narrow ** (-0.5), qb * broad ** (-0.5))
    keys = join(*pair(narrow_probe_matrix, broad_probe_matrix))
    gates = join(*pair(narrow_retention_logits, broad_retention_logits))
    extra = extra_log_retention.transpose(0, 2, 1).reshape(tok, units, 1)
    decay = jax.nn.log_sigmoid(gates) / SOFTENING + extra
    values = content_vectors.astype(F32).reshape(tok, units, dv)
    out, meets, state, fade = local_attention(query, keys, values, decay)
    packed = jnp.concatenate(
        [
            state.transpose(1, 0, 2).reshape(dv, units * broad),
            fade.reshape(1, units * broad),
            jnp.zeros((15, units * broad), F32),
        ],
        axis=0,
    ).astype(BF16)
    weights = jnp.stack(
        [content_expansion_matrix.T, switch_expansion_matrix.T, contraction_matrix], axis=0
    )
    ff = contraction_matrix.shape[0]
    half = ff // 2
    dblk = contraction_matrix.shape[1]
    q = (lax.axis_index("sp") // 2) % 2
    taps = lax.dynamic_slice_in_dim(convolution_kernel, q * half, half, axis=2)
    taps = jnp.pad(taps.astype(F32).transpose(1, 0, 2).reshape(6, half), ((0, 2), (0, 0)))
    gain = per_branch_scaling.astype(F32).reshape(units, dv)
    blend = channel_blend_scaling.astype(F32).reshape(1, -1)
    nz = n_sp // 2
    model = n_tp * cols
    dma = pltpu.SemaphoreType.DMA
    vmem = pl.BlockSpec(memory_space=pltpu.VMEM)
    return pl.pallas_call(
        functools.partial(kernel, n_sp, n_tp, units),
        out_shape=jax.ShapeDtypeStruct((tok, cols), BF16),
        in_specs=[vmem] * 9,
        out_specs=vmem,
        scratch_shapes=[
            pltpu.VMEM((n_sp, 3, half, dblk), BF16),
            pltpu.VMEM((n_sp,) + packed.shape, BF16),
            pltpu.VMEM((dv, units * broad), F32),
            pltpu.VMEM((n_tp, tok, units * dv), BF16),
            pltpu.VMEM((n_tp, tok, cols), BF16),
            pltpu.VMEM((2, tok + HALO, model), BF16),
            pltpu.VMEM((2, 2, tok + HALO, half), F32),
            pltpu.VMEM((2 * tok, half), BF16),
            pltpu.VMEM((n_tp, 2, tok, cols), BF16),
            pltpu.VMEM((2 * n_tp, tok, cols), BF16),
            dma,
            dma((n_sp,)), dma((n_sp,)),
            dma((nz,)), dma((nz,)), dma((nz,)), dma((nz,)),
            dma((nz,)), dma((nz,)), dma((nz,)), dma((nz,)),
            dma((n_tp,)), dma((n_tp,)), dma((n_tp,)), dma((n_tp,)),
            dma((3,)), dma((3,)), dma((2 * n_tp,)), dma((2 * n_tp,)),
        ],
        compiler_params=pltpu.CompilerParams(
            collective_id=0, has_side_effects=True, vmem_limit_bytes=56 * 1024 * 1024
        ),
    )(weights, packed, out, meets, gain, skip_stream, final_projection_matrix, blend, taps)


def solution(mesh):
    in_specs = (
        P("sp", "tp"),
        P("sp", "tp"),
        P("sp", "tp"),
        P("sp", "tp"),
        P("sp", "tp"),
        P("sp", "tp"),
        P("sp", "tp"),
        P("sp", "tp", None, None),
        P("sp", None, "tp"),
        P("tp", None, None),
        P(None, "tp"),
        P(),
        P("sp", "tp"),
        P("sp", "tp"),
        P(None, None, "tp"),
        P("tp", "sp"),
    )
    out_specs = P("sp", "tp")
    body = functools.partial(local, mesh.shape["sp"], mesh.shape["tp"])
    return jax.shard_map(body, mesh=mesh, in_specs=in_specs, out_specs=out_specs, check_vma=False)
```

profile of v0, /device:TPU:16, one launch (start us, length us, event | category | flops | bytes accessed | tf_op | source)
XLA Modules:
  0.0 183.5 jit_solution(9016748321535564982)
XLA Ops:
  0.0 0.0 copy-start
  0.0 1.4 copy.31
  1.5 1.4 copy.30
  2.8 0.0 copy-done.1
  2.9 0.0 copy-start.5
  2.9 0.0 copy-start.9
  2.9 0.0 copy-start.10
  2.9 0.0 copy-start.6
  2.9 0.0 copy-start.2
  2.9 0.0 copy-start.3
  2.9 1.6 pad_maximum_fusion.w_ref
  4.5 0.0 copy-done.5
  4.5 0.1 copy.32
  4.7 0.0 copy-done.9
  4.7 0.1 add.65
  4.8 0.0 copy-done.10
  4.8 0.4 fusion.14
  5.3 0.0 copy-done.6
  5.3 0.1 copy.45
  5.4 0.0 copy-done.2
  5.5 0.0 copy-done.3
  5.5 0.6 convolution_bitcast_fusion
  6.1 0.2 fusion.24
  6.3 0.1 copy.44
  6.4 0.1 pad.31.clone
  6.5 0.7 maximum_maximum_fusion.st_ref
  7.2 0.0 copy-done.4
  7.2 0.0 copy-done.7
  7.3 0.1 copy.46
  7.4 0.1 fusion.13
  7.5 0.2 copy.40
  7.7 0.6 convolution_select_fusion
  8.3 0.0 copy-start.11
  8.3 0.0 copy-start.8
  8.3 0.3 fusion.28
  8.6 0.2 multiply_add_fusion
  8.8 0.6 fusion
  9.4 0.2 copy.39
  9.6 0.8 copy_bitcast_fusion
  10.5 0.0 copy-done.11
  10.5 0.5 bitcast_convert_fusion.gain_ref
  11.0 0.0 copy-done.8
  11.0 0.6 reshape.120
  11.6 0.0 copy-done
  11.6 0.1 dynamic-slice_bitcast_fusion
  11.7 0.6 pad_convert_fusion.taps_ref
  12.3 169.5 %shard_map.154 = bf16[256,512]{1,0:T(8,128)(2,1)} custom-call(bf16[3,1408,256]{2,1,0:T(8,128)(2,1)} %pad_maximum_fusion.w_ref, bf16[144,256]{1,0:T(8,128)(2,1)} %maximum_maximum_fusion.st_ref, f32[256,256]{1,0:T(8,128)} %get-tuple-element.16.out_ref0, f32[256,256]{1,0:T(8,128)} %get-tuple-element.15.meets_ref, f32[2,128]{1,0:T(2,128)} %bitcast_convert_fusion.gain_ref, ...), custom_call_target="tpu_custom_call" | custom-call | tf_op jit(solution)/shard_map/pallas_call | solution.py:347
  181.9 1.7 copy.65
  (19 shorter events, 0.2 us)
Async XLA Ops:
  0.0 11.6 %copy-start = (bf16[3,2,1408]{2,1,0:T(2,128)(2,1)S(1)}, bf16[3,2,1408]{2,1,0:T(2,128)(2,1)}, u32[]{:S(2)}) copy-start(bf16[3,2,1408]{2,1,0:T(2,128)(2,1)} %param.30) | copy-start | bytes 50692
  0.0 2.8 %copy-start.1 = (bf16[1408,256]{1,0:T(8,128)(2,1)S(1)}, bf16[1408,256]{1,0:T(8,128)(2,1)}, u32[]{:S(2)}) copy-start(bf16[1408,256]{1,0:T(8,128)(2,1)} %param.31) | copy-start | bytes 2162692
  2.9 1.7 copy-start.5
  2.9 1.8 copy-start.9
  2.9 1.9 %copy-start.10 = (bf16[256,128]{1,0:T(8,128)(2,1)S(1)}, bf16[256,128]{1,0:T(8,128)(2,1)}, u32[]{:S(2)}) copy-start(bf16[256,128]{1,0:T(8,128)(2,1)} %param.22) | copy-start | bytes 196612
  2.9 2.4 %copy-start.6 = (bf16[256,64]{0,1:T(8,128)(2,1)S(1)}, bf16[256,64]{0,1:T(8,128)(2,1)}, u32[]{:S(2)}) copy-start(bf16[256,64]{0,1:T(8,128)(2,1)} %param.18) | copy-start | bytes 98308
  2.9 2.5 %copy-start.2 = (bf16[256,1,2,128]{3,2,1,0:T(2,128)(2,1)S(1)}, bf16[256,1,2,128]{3,2,1,0:T(2,128)(2,1)}, u32[]{:S(2)}) copy-start(bf16[256,1,2,128]{3,2,1,0:T(2,128)(2,1)} %param.23) | copy-start | bytes 393220
  2.9 2.5 %copy-start.3 = (bf16[256,128]{1,0:T(8,128)(2,1)S(1)}, bf16[256,128]{1,0:T(8,128)(2,1)}, u32[]{:S(2)}) copy-start(bf16[256,128]{1,0:T(8,128)(2,1)} %param.21) | copy-start | bytes 196612
  4.5 2.7 %copy-start.4 = (bf16[256,128]{1,0:T(8,128)(2,1)S(1)}, bf16[256,128]{1,0:T(8,128)(2,1)}, u32[]{:S(2)}) copy-start(bf16[256,128]{1,0:T(8,128)(2,1)} %param.20) | copy-start | bytes 196612
  4.5 2.7 %copy-start.7 = (bf16[256,64]{0,1:T(8,128)(2,1)S(1)}, bf16[256,64]{0,1:T(8,128)(2,1)}, u32[]{:S(2)}) copy-start(bf16[256,64]{0,1:T(8,128)(2,1)} %param.17) | copy-start | bytes 98308
  8.3 2.2 %copy-start.11 = (bf16[1,2,128]{2,1,0:T(2,128)(2,1)S(1)}, bf16[1,2,128]{2,1,0:T(2,128)(2,1)}, u32[]{:S(2)}) copy-start(bf16[1,2,128]{2,1,0:T(2,128)(2,1)} %param.25) | copy-start | bytes 1540
  8.3 2.7 %copy-start.8 = (bf16[2048]{0:T(1024)(128)(2,1)S(1)}, bf16[2048]{0:T(1024)(128)(2,1)}, u32[]{:S(2)}) copy-start(bf16[2048]{0:T(1024)(128)(2,1)} %param.27) | copy-start | bytes 12292
where the time goes:
time: 184 us
  Pallas kernels  170 us (92%)
  local copies, waits for them, and re-layouts  6.56 us (4%)
  other arithmetic  4.6 us (2%)
  matrix products  2.54 us (1%)
    pallas_call x1, Pallas kernels, local(): pl.pallas_call(functools.partial(kernel, n_sp, n_tp, units), out_shape=ja...  170 us
    unnamed x31, local copies, waits for them, and re-layouts  4.89 us

commit v1 on v0

v1 whole, which is shorter than its diff:
```python
import functools

import jax
import jax.numpy as jnp
from jax import lax
from jax.experimental import pallas as pl
from jax.experimental.pallas import tpu as pltpu
from jax.sharding import PartitionSpec as P

BLOCK = 64
HALO = 16
LANES = 128
GROUP = 4
EPSILON = 1e-06
SOFTENING = 16.0
HIGHEST = lax.Precision.HIGHEST
F32 = jnp.float32
BF16 = jnp.bfloat16
NT = (((1,), (1,)), ((), ()))
TN = (((0,), (0,)), ((), ()))


def exact(a, b, dims):
    return lax.dot_general(a, b, dims, precision=HIGHEST, preferred_element_type=F32)


def local_attention(
    q_refs, k_refs, g_refs, v_ref, extra_ref, out_ref, meets_ref, st_ref
):
    tok, units, dv = v_ref.shape
    key = q_refs[1].shape[1]
    dim = q_refs[0].shape[0]

    def join(refs, scale):
        first = jnp.transpose(refs[0][...].astype(F32))
        second = refs[1][...].astype(F32)
        if scale:
            first = first * dim ** (-0.5)
            second = second * key ** (-0.5)
        if dim < key:
            first = jnp.concatenate([first, jnp.zeros((tok, key - dim), F32)], axis=1)
        return jnp.concatenate([first, second], axis=1)

    gate = join(g_refs, False)
    query_all = join(q_refs, True)
    keys_all = join(k_refs, False)
    soft = jnp.minimum(gate, 0.0) - jnp.log1p(jnp.exp(-jnp.abs(gate)))
    extra = jnp.transpose(
        jnp.concatenate([extra_ref[u] for u in range(units)] + [jnp.zeros((8 - units, tok), F32)], axis=0)
    )
    decay = jnp.concatenate(
        [
            soft[:, u * key : (u + 1) * key] * (1.0 / SOFTENING) + extra[:, u : u + 1]
            for u in range(units)
        ],
        axis=1,
    )
    values_all = v_ref[...].astype(F32)
    row = lax.broadcasted_iota(jnp.int32, (BLOCK, BLOCK), 0)
    col = lax.broadcasted_iota(jnp.int32, (BLOCK, BLOCK), 1)
    lower = row >= col
    tri = jnp.where(lower, 1.0, 0.0)
    plain = (((1,), (0,)), ((), ()))
    before = jnp.zeros((1, units * key), F32)
    state = [jnp.zeros((dv, key), F32) for _ in range(units)]
    for n in range(tok // BLOCK):
        rows = slice(n * BLOCK, (n + 1) * BLOCK)
        inner = exact(tri, decay[rows], plain)
        last = inner[BLOCK - 1 : BLOCK]
        middle = inner[BLOCK // 2 - 1 : BLOCK // 2]
        query = query_all[rows]
        keys = keys_all[rows]
        query_mid = query * jnp.exp(inner - middle)
        key_mid = keys * jnp.exp(middle - inner)
        query_carry = query * jnp.exp(inner)
        key_carry = keys * jnp.exp(last - inner)
        meets_ref[rows] = query_carry * jnp.exp(before)
        gone = jnp.exp(last)
        for u in range(units):
            at = slice(u * key, (u + 1) * key)
            vu = values_all[rows, u, :]
            scores = exact(query_mid[:, at], key_mid[:, at], NT)
            out = exact(jnp.where(lower, scores, 0.0), vu, plain)
            if n:
                out = out + exact(query_carry[:, at], state[u], NT)
            out_ref[rows, u * dv : (u + 1) * dv] = out
            state[u] = gone[:, at] * state[u] + exact(vu, key_carry[:, at], TN)
        before = before + last
    fade = jnp.exp(before)
    upper = dv // 2
    st_ref[:dv] = state[1].astype(BF16)
    st_ref[dv : dv + upper] = jnp.concatenate(
        [state[0][:upper, :dim], state[0][upper:, :dim]], axis=1
    ).astype(BF16)
    fades = [fade[:, key:], jnp.concatenate([fade[:, :dim], fade[:, :dim]], axis=1)]
    st_ref[dv + upper :] = jnp.concatenate(
        fades + [jnp.zeros((HALO - units, key), F32)], axis=0
    ).astype(BF16)


def kernel(
    n_sp, n_tp,
    wv_ref, wg_ref, wd_ref, qn_ref, kn_ref, gn_ref, qb_ref, kb_ref, gb_ref, v_ref, extra_ref,
    gain_ref, skip_ref, proj_ref, blend_ref, taps_ref,
    mixed_ref,
    wup, wdn, taps, st_own, stbuf, acc_state, out0, meets, heads, piece, up,
    tail, halo, hid, psum, csum, xsum, xbuf, zsum, zbuf, acc_out,
    own_sem, st_send, st_recv, wz_send, wz_recv, wy_send, wy_recv, hx_sems, hc_send,
    hc_recv, tail_send, tail_recv, az_up, az_down, az_recv, ax_send, ax_recv, ac_send, ac_recv, rc_send,
    rc_recv, rx_send, rx_recv, rz_send, rz_recv,
):
    s, t = lax.axis_index("sp"), lax.axis_index("tp")
    nz = n_sp // 2
    z, y = s // 2, s % 2
    zi = z % GROUP
    base = z - zi
    side = s + 1 - 2 * y
    core = t % 2
    tx = lax.rem(t + n_tp // 2, n_tp)
    tc = t + 1 - 2 * core
    tok, cols = skip_ref.shape
    units = v_ref.shape[1]
    kblk, ff = wv_ref.shape
    dblk = wd_ref.shape[1]
    dv = v_ref.shape[2]
    key = qb_ref.shape[1]
    tiles = ff // LANES
    wide_tiles = -(-tiles // GROUP)
    short = wide_tiles * GROUP - tiles
    wide = wide_tiles * LANES
    narrow = wide - LANES

    def rc(src, dst, ss, rs, sp, tp):
        return pltpu.make_async_remote_copy(
            src_ref=src, dst_ref=dst, send_sem=ss, recv_sem=rs,
            device_id=(sp, tp), device_id_type=pl.DeviceIdType.MESH,
        )

    bar = pltpu.get_barrier_semaphore()
    for o in range(1, n_sp):
        pl.semaphore_signal(bar, inc=1, device_id=(lax.rem(s + o, n_sp), t),
                            device_id_type=pl.DeviceIdType.MESH)
    for o in range(1, n_tp):
        pl.semaphore_signal(bar, inc=1, device_id=(s, lax.rem(t + o, n_tp)),
                            device_id_type=pl.DeviceIdType.MESH)
    pl.semaphore_wait(bar, n_sp + n_tp - 2)

    def share(member):
        at = jnp.maximum(member * wide_tiles - core * short, 0)
        thin = jnp.where(core == 0, GROUP - 1, 0)
        return pl.multiple_of(at * LANES, LANES), member == thin

    def each_width(thin, fn):
        if short == 0:
            fn(wide)
            return

        @pl.when(jnp.logical_not(thin))
        def _():
            fn(wide)

        @pl.when(thin)
        def _():
            fn(narrow)

    my_at, my_thin = share(zi)

    def fitting(at, width):
        return pl.multiple_of(jnp.minimum(at, ff - width), LANES)

    def source(m, at, width):
        at = fitting(at, width)
        if m == 2:
            return wd_ref.at[pl.ds(at, width)]
        return (wv_ref, wg_ref)[m].at[:, pl.ds(at, width)]

    def place(m, slot, width):
        if m == 2:
            return wdn.at[slot, pl.ds(0, width)]
        rows = pl.ds(pl.multiple_of(slot * kblk, HALO), kblk)
        return wup.at[rows, pl.ds(m * wide, width)]

    def zcopy(m, o, width):
        zz = lax.rem(z + o, nz)
        at, _ = share(zz % GROUP)
        return rc(source(m, at, width), place(m, s, width), wz_send.at[m, o], wz_recv.at[m, o],
                  zz * 2 + y, t)

    def ycopy(m, o, width):
        slot = lax.rem(z + nz - o, nz) * 2 + y
        first = isinstance(o, int) and o == 0
        src = source(m, my_at, width) if first else place(m, slot, width)
        return rc(src, place(m, slot, width), wy_send.at[m, o], wy_recv.at[m, o], side, t)

    def own(m, width):
        return pltpu.make_async_copy(source(m, my_at, width), place(m, s, width), own_sem.at[m])

    def thin_of(o):
        return share(lax.rem(z + o, nz) % GROUP)[1]

    ranks = ((0, 1, 2, 3), (1, 0, 2, 3), (2, 1, 3, 0), (3, 2, 1, 0))

    def member(o):
        j = jnp.int32(0)
        for r in range(GROUP):
            j = jnp.where(zi == r, ranks[r][o], j)
        return j

    def launch_z(m):
        for o in range(1, nz):
            each_width(thin_of(o), lambda w, o=o: zcopy(m, o, w).start())

    def launch_way(m, upward, where=True):
        for o in range(1, nz):
            way = z + o < nz if upward else z + o >= nz

            @pl.when(jnp.logical_and(way, where))
            def _(o=o):
                each_width(thin_of(o), lambda w: zcopy(m, o, w).start())

    def launch_y(m):
        each_width(my_thin, lambda w: ycopy(m, 0, w).start())

    def relay(m, turns=(1, 2, 3)):
        if nz == GROUP:
            offsets = [lax.rem(zi + GROUP - member(k), GROUP) for k in turns]
        else:
            offsets = range(1, nz) if 1 in turns else ()
        for o in offsets:
            def go(w, o=o):
                zcopy(m, o, w).wait_recv()
                ycopy(m, o, w).start()
            each_width(my_thin, go)

    def settle(m):
        def go(w):
            own(m, w).wait()
            for o in range(nz):
                ycopy(m, o, w).wait_recv()
        each_width(my_thin, go)

    for m in range(3):
        each_width(my_thin, lambda w, m=m: own(m, w).start())
    launch_z(0)
    launch_y(0)
    launch_y(1)
    taps[...] = jnp.zeros_like(taps)

    def load_taps(width):
        for m in range(2):
            for i in range(3):
                taps[m * 3 + i : m * 3 + i + 1, :width] = taps_ref[
                    i, m : m + 1, pl.ds(fitting(my_at, width), width)
                ].astype(F32)
    each_width(my_thin, load_taps)
    if short:
        @pl.when(my_thin)
        def _():
            for m in range(2):
                wup[:, m * wide + narrow : (m + 1) * wide] = jnp.zeros((n_sp * kblk, LANES), BF16)
            for i in range(n_sp):
                wdn[i, narrow:] = jnp.zeros((LANES, dblk), BF16)

    local_attention(
        (qn_ref, qb_ref), (kn_ref, kb_ref), (gn_ref, gb_ref), v_ref, extra_ref, out0, meets, st_own
    )
    st = [None] + [
        rc(st_own, stbuf.at[s], st_send.at[o], st_recv.at[o], lax.rem(s + o, n_sp), t)
        for o in range(1, n_sp)
    ]
    for o in range(1, n_sp):
        @pl.when(s + o < n_sp)
        def _(o=o):
            st[o].start()
    launch_way(1, False)

    acc_state[...] = jnp.zeros_like(acc_state)
    for o in range(n_sp - 1, 0, -1):
        @pl.when(s - o >= 0)
        def _(o=o):
            st[o].wait_recv()
            got = stbuf[s - o].astype(F32)
            fade = dv + dv // 2
            acc_state[:dv] = got[fade : fade + 1] * acc_state[:dv] + got[:dv]
            acc_state[dv:] = got[fade + 1 : fade + 2] * acc_state[dv:] + got[dv:fade]
    for u in range(units):
        at = slice(u * dv, (u + 1) * dv)
        ku = slice(u * key, (u + 1) * key)
        if u:
            total = out0[:, at] + exact(meets[:, ku], acc_state[:dv], NT)
        else:
            dim = qn_ref.shape[0]
            folded = jnp.concatenate([acc_state[dv:, :dim], acc_state[dv:, dim:]], axis=0)
            total = out0[:, at] + exact(meets[:, :dim], folded, NT)
        scale = lax.rsqrt(jnp.mean(total * total, axis=-1, keepdims=True) + EPSILON)
        heads[t, :, at] = (total * scale * gain_ref[0, u : u + 1].astype(F32)).astype(BF16)
    tcx = lax.rem(tc + n_tp // 2, n_tp)
    hx = rc(heads.at[t], heads.at[t], hx_sems.at[0], hx_sems.at[1], s, tx)
    hc = [
        rc(heads.at[slot], heads.at[slot], hc_send.at[i], hc_recv.at[i], s, tc)
        for i, slot in enumerate((t, tx))
    ]
    hx.start()
    hc[0].start()
    relay(0, (1,))
    hx.wait_recv()
    hc[1].start()
    for copy in hc:
        copy.wait_recv()
    whole_heads = jnp.concatenate([heads[i] for i in range(n_tp)], axis=1)
    projected = skip_ref[...].astype(F32) + jnp.dot(
        whole_heads, proj_ref[...], preferred_element_type=F32
    )
    piece[zi, t] = projected.astype(BF16)

    def above(j):
        return rc(piece.at[j, t], piece.at[j, t], az_up.at[j], az_recv.at[j],
                  jnp.where(zi < GROUP - 1, s + 2, s), t)

    def below(j):
        return rc(piece.at[j, t], piece.at[j, t], az_down.at[j], az_recv.at[j],
                  jnp.where(zi > 0, s - 2, s), t)

    def spread(j, up_act, down_act):
        @pl.when(jnp.logical_and(j <= zi, zi < GROUP - 1))
        def _():
            up_act(above(j))

        @pl.when(jnp.logical_and(j >= zi, zi > 0))
        def _():
            down_act(below(j))

    def across(o, tp_slot, ss, rs, to):
        j = member(o)
        return rc(piece.at[j, tp_slot], piece.at[j, tp_slot], ss, rs, s, to)

    ax = [across(o, t, ax_send.at[o], ax_recv.at[o], tx) for o in range(GROUP)]
    ax_got = [across(o, tx, ax_send.at[o], ax_recv.at[o], tx) for o in range(GROUP)]
    ac = [
        [across(o, slot, ac_send.at[o, i], ac_recv.at[o, i], tc) for i, slot in enumerate((t, tx))]
        for o in range(GROUP)
    ]
    ac_got = [
        [across(o, slot, ac_send.at[o, i], ac_recv.at[o, i], tc)
         for i, slot in enumerate((tc, tcx))]
        for o in range(GROUP)
    ]
    def begin(copy):
        copy.start()

    def finish(copy):
        copy.wait_send()

    def collect(o):
        j = member(o)
        above(j).wait_recv()
        spread(j, begin, begin)
        ax[o].start()
        ac[o][0].start()

    ax[0].start()
    spread(zi, begin, begin)
    ac[0][0].start()
    def exchange(o):
        ax_got[o].wait_recv()
        ac[o][1].start()

    @pl.when(zi == 1)
    def _():
        collect(1)

    launch_way(1, True, zi == 1)
    relay(0, (2, 3))
    launch_y(2)

    @pl.when(zi != 1)
    def _():
        collect(1)

    launch_way(1, True, jnp.logical_or(zi == 0, zi == GROUP - 1))
    exchange(0)
    collect(2)
    exchange(1)
    collect(3)
    launch_way(1, True, zi == 2)
    launch_way(2, True)
    launch_way(2, False)
    relay(1, (1, 2, 3))
    exchange(2)
    exchange(3)

    def expand(o):
        j = member(o)
        squares = jnp.zeros((tok, 1), F32)
        for i in range(n_tp):
            part = piece[j, i].astype(F32)
            squares = squares + jnp.sum(part * part, axis=1, keepdims=True)
        scale = lax.rsqrt(squares / (n_tp * cols) + EPSILON)
        total = None
        for i in range(n_tp):
            at = slice(i * cols, (i + 1) * cols)
            normed = (piece[j, i].astype(F32) * scale * blend_ref[:, at]).astype(BF16)
            part = jnp.dot(normed, wup[at], preferred_element_type=F32)
            total = part if total is None else total + part
        rounded = total.astype(BF16)
        tail[o] = rounded[tok - HALO :]
        up[o, HALO:] = rounded.astype(F32)

    def tail_copy(o, slot, to_sp):
        return rc(tail.at[o], halo.at[slot], tail_send.at[o], tail_recv.at[slot], to_sp, t)

    def tail_route(o, act):
        j = member(o)

        @pl.when(y == 0)
        def _():
            act(tail_copy(o, j, side))

        @pl.when(jnp.logical_and(y == 1, j < GROUP - 1))
        def _():
            act(tail_copy(o, jnp.minimum(j + 1, GROUP - 1), side))

        if nz > GROUP:
            @pl.when(jnp.logical_and(jnp.logical_and(y == 1, j == GROUP - 1), z + GROUP < nz))
            def _():
                act(tail_copy(o, 0, jnp.minimum(z + GROUP, nz - 1) * 2))

    def convolve(o):
        j = member(o)
        fresh = jnp.logical_and(jnp.logical_and(y == 0, j == 0), z < GROUP)

        @pl.when(fresh)
        def _():
            up[o, :HALO] = jnp.zeros((HALO, 2 * wide), F32)

        @pl.when(jnp.logical_not(fresh))
        def _():
            tail_copy(o, j, side).wait_recv()
            up[o, :HALO] = halo[j].astype(F32)
        conv = []
        for m in range(2):
            at = slice(m * wide, (m + 1) * wide)
            sums = taps[m * 3 : m * 3 + 1] * up[o, pl.ds(HALO - 2, tok), at]
            sums += taps[m * 3 + 1 : m * 3 + 2] * up[o, pl.ds(HALO - 1, tok), at]
            sums += taps[m * 3 + 2 : m * 3 + 3] * up[o, pl.ds(HALO, tok), at]
            conv.append(sums)
        value, gate = conv
        hid[o] = (gate / (1.0 + jnp.exp(-gate)) * value).astype(BF16)

    settle(0)
    settle(1)
    for o in range(GROUP):
        for copy in ac_got[o]:
            copy.wait_recv()
        expand(o)
        tail_route(o, begin)
        if o:
            relay(2, (o,))
    settle(2)

    per = cols // dblk
    half = n_tp // 2
    order = [3, 2, 1, 0]

    def contract(o):
        for i in range(n_tp):
            for j in range(per):
                psum[o, i, :, j * dblk : (j + 1) * dblk] = jnp.dot(
                    hid[o], wdn[i * per + j], preferred_element_type=F32
                ).astype(BF16)

    rcc = [
        [rc(psum.at[o, i * 2 + 1 - core], csum.at[o, i], rc_send.at[o, i], rc_recv.at[o, i], s, tc)
         for i in range(half)]
        for o in range(GROUP)
    ]
    rx = [rc(xsum.at[o], xbuf.at[o], rx_send.at[o], rx_recv.at[o], s, tx) for o in range(GROUP)]
    def rise(j):
        return rc(zsum.at[j], zbuf.at[0, j], rz_send.at[j], rz_recv.at[0, j],
                  jnp.where(zi < GROUP - 1, s + 2, s), t)

    def fall(j):
        return rc(zsum.at[j], zbuf.at[1, j], rz_send.at[j], rz_recv.at[1, j],
                  jnp.where(zi > 0, s - 2, s), t)

    mine = t // 2
    for step in range(GROUP + 1):
        if step < GROUP:
            o = order[step]
            convolve(o)
            contract(o)
            for copy in rcc[o]:
                copy.start()
        if step:
            o = order[step - 1]
            for copy in rcc[o]:
                copy.wait_recv()
            theirs = half - 1 - mine
            xsum[o] = (psum[o, theirs * 2 + core].astype(F32) + csum[o, theirs].astype(F32)).astype(
                BF16
            )
            rx[o].start()
    def reduced(o):
        return psum[o, t].astype(F32) + csum[o, mine].astype(F32) + xbuf[o].astype(F32)

    for o in order[:-1]:
        j = member(o)
        rx[o].wait_recv()

        @pl.when(j > zi)
        def _(o=o, j=j):
            @pl.when(zi > 0)
            def _():
                rise(j).wait_recv()
                zsum[j] = (reduced(o) + zbuf[0, j].astype(F32)).astype(BF16)

            @pl.when(zi == 0)
            def _():
                zsum[j] = reduced(o).astype(BF16)
            rise(j).start()

        @pl.when(j < zi)
        def _(o=o, j=j):
            @pl.when(zi < GROUP - 1)
            def _():
                fall(j).wait_recv()
                zsum[j] = (reduced(o) + zbuf[1, j].astype(F32)).astype(BF16)

            @pl.when(zi == GROUP - 1)
            def _():
                zsum[j] = reduced(o).astype(BF16)
            fall(j).start()
    rx[0].wait_recv()
    acc_out[...] = reduced(0) + piece[zi, t].astype(F32)

    @pl.when(zi > 0)
    def _():
        rise(zi).wait_recv()
        acc_out[...] += zbuf[0, zi].astype(F32)

    @pl.when(zi < GROUP - 1)
    def _():
        fall(zi).wait_recv()
        acc_out[...] += zbuf[1, zi].astype(F32)
    mixed_ref[...] = acc_out[...].astype(BF16)

    for o in range(1, n_sp):
        @pl.when(s + o < n_sp)
        def _(o=o):
            st[o].wait_send()

    for m in range(3):
        for o in range(1, nz):
            each_width(thin_of(o), lambda w, m=m, o=o: zcopy(m, o, w).wait_send())

        def drain(w, m=m):
            for o in range(nz):
                ycopy(m, o, w).wait_send()
        each_width(my_thin, drain)
    for o in range(GROUP):
        tail_route(o, finish)
        spread(member(o), finish, finish)
    for o in order[:-1]:
        rise(member(o)).wait_send()
    for copy in [hx] + hc + ax + rx:
        copy.wait_send()
    for o in range(GROUP):
        for copy in ac[o] + rcc[o]:
            copy.wait_send()


def local(
    n_sp, n_tp,
    skip_stream,
    narrow_lookup_matrix,
    narrow_probe_matrix,
    narrow_retention_logits,
    broad_lookup_matrix,
    broad_probe_matrix,
    broad_retention_logits,
    content_vectors,
    extra_log_retention,
    per_branch_scaling,
    final_projection_matrix,
    channel_blend_scaling,
    switch_expansion_matrix,
    content_expansion_matrix,
    convolution_kernel,
    contraction_matrix,
):
    tok, cols = skip_stream.shape
    heads = content_vectors.shape[1]
    dv = content_vectors.shape[3]
    narrow = narrow_lookup_matrix.shape[1]
    broad = broad_lookup_matrix.shape[1]
    units = 2 * heads
    kblk, ff = content_expansion_matrix.shape
    dblk = contraction_matrix.shape[1]
    assert heads == 1 and n_tp == 4 and 2 * narrow == broad
    values = content_vectors.reshape(tok, units, dv)
    extra = extra_log_retention.transpose(1, 2, 0)
    blend = channel_blend_scaling.astype(F32).reshape(1, -1)
    wide = -(-(ff // LANES) // GROUP) * LANES
    nz = n_sp // 2
    width = units * broad
    model = n_tp * cols
    dma = pltpu.SemaphoreType.DMA
    vmem = pl.BlockSpec(memory_space=pltpu.VMEM)
    anywhere = pl.BlockSpec(memory_space=pltpu.HBM)
    return pl.pallas_call(
        functools.partial(kernel, n_sp, n_tp),
        out_shape=jax.ShapeDtypeStruct((tok, cols), BF16),
        in_specs=[anywhere] * 3 + [vmem] * 13,
        out_specs=vmem,
        scratch_shapes=[
            pltpu.VMEM((model, 2 * wide), BF16),
            pltpu.VMEM((n_sp, wide, dblk), BF16),
            pltpu.VMEM((8, wide), F32),
            pltpu.VMEM((dv + dv // 2 + HALO, broad), BF16),
            pltpu.VMEM((n_sp, dv + dv // 2 + HALO, broad), BF16),
            pltpu.VMEM((dv + dv // 2, broad), F32),
            pltpu.VMEM((tok, units * dv), F32),
            pltpu.VMEM((tok, width), F32),
            pltpu.VMEM((n_tp, tok, units * dv), BF16),
            pltpu.VMEM((GROUP, n_tp, tok, cols), BF16),
            pltpu.VMEM((GROUP, HALO + tok, 2 * wide), F32),
            pltpu.VMEM((GROUP, HALO, 2 * wide), BF16),
            pltpu.VMEM((GROUP, HALO, 2 * wide), BF16),
            pltpu.VMEM((GROUP, tok, wide), BF16),
            pltpu.VMEM((GROUP, n_tp, tok, cols), BF16),
            pltpu.VMEM((GROUP, n_tp // 2, tok, cols), BF16),
            pltpu.VMEM((GROUP, tok, cols), BF16),
            pltpu.VMEM((GROUP, tok, cols), BF16),
            pltpu.VMEM((GROUP, tok, cols), BF16),
            pltpu.VMEM((2, GROUP, tok, cols), BF16),
            pltpu.VMEM((tok, cols), F32),
            dma((3,)),
            dma((n_sp,)), dma((n_sp,)),
            dma((3, nz)), dma((3, nz)), dma((3, nz)), dma((3, nz)),
            dma((2,)), dma((2,)), dma((2,)), dma((GROUP,)), dma((GROUP,)),
            dma((GROUP,)), dma((GROUP,)), dma((GROUP,)), dma((GROUP,)), dma((GROUP,)),
            dma((GROUP, 2)), dma((GROUP, 2)), dma((GROUP, 2)), dma((GROUP, 2)),
            dma((GROUP,)), dma((GROUP,)), dma((GROUP,)), dma((2, GROUP)),
        ],
        compiler_params=pltpu.CompilerParams(
            collective_id=0, has_side_effects=True, vmem_limit_bytes=58 * 1024 * 1024
        ),
    )(
        content_expansion_matrix, switch_expansion_matrix, contraction_matrix, narrow_lookup_matrix.T,
        narrow_probe_matrix.T, narrow_retention_logits.T, broad_lookup_matrix, broad_probe_matrix,
        broad_retention_logits, values, extra, per_branch_scaling, skip_stream,
        final_projection_matrix, blend, convolution_kernel,
    )


def solution(mesh):
    in_specs = (
        P("sp", "tp"),
        P("sp", "tp"),
        P("sp", "tp"),
        P("sp", "tp"),
        P("sp", "tp"),
        P("sp", "tp"),
        P("sp", "tp"),
        P("sp", "tp", None, None),
        P("sp", None, "tp"),
        P("tp", None, None),
        P(None, "tp"),
        P(),
        P("sp", "tp"),
        P("sp", "tp"),
        P(None, None, "tp"),
        P("tp", "sp"),
    )
    out_specs = P("sp", "tp")
    body = functools.partial(local, mesh.shape["sp"], mesh.shape["tp"])
    return jax.shard_map(body, mesh=mesh, in_specs=in_specs, out_specs=out_specs, check_vma=False)
```

time: 184 us -> 132 us (0.72)
  the two profiles are of different devices: /device:TPU:16 before, /device:TPU:0 now
where the time goes in v1:
time: 132 us
  Pallas kernels  129 us (98%)
  local copies, waits for them, and re-layouts  2.36 us (2%)
    pallas_call x1, Pallas kernels, local(): pl.pallas_call(functools.partial(kernel, n_sp, n_tp), out_shape=jax.Shape...  129 us

profile of v1, /device:TPU:0, one launch (start us, length us, event | category | flops | bytes accessed | tf_op | source)
XLA Modules:
  0.0 131.7 jit_solution(15380632523865578967)
XLA Ops:
  0.0 0.0 copy-start
  0.0 0.7 copy-done
  0.7 0.6 reshape.11
  1.3 128.7 %shard_map.154 = bf16[256,512]{1,0:T(8,128)(2,1)} custom-call(bf16[256,1408]{1,0:T(8,128)(2,1)} %wv_ref.1, bf16[256,1408]{1,0:T(8,128)(2,1)} %wg_ref.1, bf16[1408,256]{1,0:T(8,128)(2,1)} %wd_ref.1, bf16[64,256]{1,0:T(8,128)(2,1)} %bitcast.7, bf16[64,256]{1,0:T(8,128)(2,1)} %bitcast.8, bf16[64,256]{1,0:T(8,128)(2,1)} %bitcast.9, bf16[256,128]{1,0:T(8,128)(2,1)} %qb_ref.1, ...), custom_call_target="tpu_custom_call" | custom-call | tf_op jit(solution)/shard_map/pallas_call | solution.py:610
  130.0 1.7 %copy.18 = bf16[256,512]{1,0:T(8,128)(2,1)} copy(bf16[256,512]{1,0:T(8,128)(2,1)} %shard_map.154) | data formatting | bytes 524288
Async XLA Ops:
  0.0 0.7 copy-start

commit v2 on v1

--- a/solution.py
+++ b/solution.py
@@ -378,14 +378,41 @@
         collect(1)
 
     launch_way(1, True, jnp.logical_or(zi == 0, zi == GROUP - 1))
+    launch_way(2, True, zi == 0)
+    launch_way(1, True, zi == 2)
     exchange(0)
+
+    @pl.when(zi == 0)
+    def _():
+        relay(1, (1,))
+
+    @pl.when(jnp.logical_or(zi == 1, zi == 2))
+    def _():
+        relay(1, (2,))
+
     collect(2)
     exchange(1)
+
+    @pl.when(zi == 0)
+    def _():
+        relay(1, (2,))
+
+    @pl.when(zi == 1)
+    def _():
+        relay(1, (3,))
+
+    @pl.when(zi == GROUP - 1)
+    def _():
+        relay(1, (1,))
+
     collect(3)
-    launch_way(1, True, zi == 2)
-    launch_way(2, True)
+    launch_way(2, True, zi > 0)
     launch_way(2, False)
-    relay(1, (1, 2, 3))
+    for r, turns in enumerate(((3,), (1,), (1, 3), (2, 3))):
+        @pl.when(zi == r)
+        def _(turns=turns):
+            relay(1, turns)
+
     exchange(2)
     exchange(3)
 
@@ -449,13 +476,22 @@
 
     settle(0)
     settle(1)
+    def relay_down(plan):
+        for r, turns in plan.items():
+            @pl.when(zi == r)
+            def _(turns=turns):
+                relay(2, turns)
+
+    down_plan = (
+        {0: (3,), 3: (2,)}, {1: (1,), 2: (1,), 3: (3,)}, {1: (2,), 2: (2,)}, {1: (3,), 2: (3,)}
+    )
+    relay_down({0: (1, 2), 3: (1,)})
     for o in range(GROUP):
         for copy in ac_got[o]:
             copy.wait_recv()
         expand(o)
         tail_route(o, begin)
-        if o:
-            relay(2, (o,))
+        relay_down(down_plan[o])
     settle(2)
 
     per = cols // dblk

time: 132 us -> 128 us (0.970); the launches traced: 132 us -> 126 us
  Pallas kernels: 129 us -> 123 us
    pallas_call x1, Pallas kernels: 129 us -> 123 us  [local(): pl.pallas_call(functools.partial(kernel, n_sp, n_tp), out_shape=jax.Shape...]
where the time goes in v2:
time: 128 us; the launch traced here: 126 us
  Pallas kernels  123 us (96%)
  local copies, waits for them, and re-layouts  2.36 us (2%)
    pallas_call x1, Pallas kernels, local(): pl.pallas_call(functools.partial(kernel, n_sp, n_tp), out_shape=jax.Shape...  123 us

profile of v2, /device:TPU:0, one launch (start us, length us, event | category | flops | bytes accessed | tf_op | source)
XLA Modules:
  0.0 126.1 jit_solution(14843146404945181700)
XLA Ops:
  0.0 0.0 copy-start
  0.0 0.7 copy-done
  0.7 0.6 reshape.11
  1.3 123.1 %shard_map.154 = bf16[256,512]{1,0:T(8,128)(2,1)} custom-call(bf16[256,1408]{1,0:T(8,128)(2,1)} %wv_ref.1, bf16[256,1408]{1,0:T(8,128)(2,1)} %wg_ref.1, bf16[1408,256]{1,0:T(8,128)(2,1)} %wd_ref.1, bf16[64,256]{1,0:T(8,128)(2,1)} %bitcast.7, bf16[64,256]{1,0:T(8,128)(2,1)} %bitcast.8, bf16[64,256]{1,0:T(8,128)(2,1)} %bitcast.9, bf16[256,128]{1,0:T(8,128)(2,1)} %qb_ref.1, ...), custom_call_target="tpu_custom_call" | custom-call | tf_op jit(solution)/shard_map/pallas_call | solution.py:646
  124.4 1.7 %copy.18 = bf16[256,512]{1,0:T(8,128)(2,1)} copy(bf16[256,512]{1,0:T(8,128)(2,1)} %shard_map.154) | data formatting | bytes 524288
Async XLA Ops:
  0.0 0.7 copy-start
